TPU v7x, 256 devices: a 8x8x2 block of a 8x8x16 slice. The times are simulated.
256 devices in a mesh: grp: 2 (over z), st: 16 (over y, core), tp: 8 (over x).
Axes of the slice: x: 8, y: 8, z: 2, core: 2. Of those that a mesh axis runs over, the one named last changes fastest.
The devices are a block of a 8x8x16 slice.
Arguments:
- tokens: bfloat16 [8192, 2048], P(('grp', 'st')), parts along dimension 0, may hold values from -6 to 6
- pre_gain: float32 [2048], replicated, may hold values from 0.1 to 1.9
- w_gated: bfloat16 [2048, 1536], P(None, 'tp'), may hold values from -0.125 to 0.125
- w_mixed: bfloat16 [2048, 1536], P(None, 'tp'), may hold values from -0.125 to 0.125
- mix_weight: bfloat16 [8, 128, 128], P('tp'), may hold values from -0.5 to 0.5
- w_query: bfloat16 [2048, 1024], P(None, 'tp'), may hold values from -0.125 to 0.125
- w_gate_mix: bfloat16 [2048, 1536], P(None, 'tp'), may hold values from -0.125 to 0.125
- w_gate_read: bfloat16 [2048, 1024], P(None, 'tp'), may hold values from -0.125 to 0.125
- store: bfloat16 [256, 128, 2048], P(('grp', 'st')), parts along dimension 0, may hold values from -6 to 6
- mem_gain: float32 [2048], replicated, may hold values from 1 to 80
- w_key: bfloat16 [2048, 1024], P(None, 'tp'), may hold values from -0.125 to 0.125
- w_value: bfloat16 [2048, 1024], P(None, 'tp'), may hold values from -0.125 to 0.125
- passage_ids: int32 [128, 4], P(('grp', 'st')), parts along dimension 0, may hold values from 0 to 127, as said below
- w_out_mix: bfloat16 [1536, 2048], P('tp'), may hold values from -0.125 to 0.125
- w_out_read: bfloat16 [1024, 2048], P('tp'), may hold values from -0.125 to 0.125
Outputs:
- mixed_out: bfloat16 [8192, 2048], P(('grp', 'st', 'tp')), parts along dimension 0
There are 2 independent parts, one for each index of `grp`. A program takes and returns all parts, laid end to end along the dimension named above; an argument that names none is the same for every part. Nothing has to cross between parts.
Inputs may be any that keep to these rules, and one draw needn't show every extreme that they name: `passage_ids`: passage p is held by index p // 8 of st. The 16 entries of one index of st name at most 2 passages held by any one index of st, and that most is reached in every draw.
All inputs are finite; a program needn't handle non-finite values.
Results may differ from a plain program's by a relative error of at most 0.015.
The roundings to bfloat16 on the way count: a program that leaves them out, or rounds other values in their place, can miss the bound.
Values may be sent and summed in bfloat16 or wider, within the bound.
A program may use at most 128 MiB of HBM per device.

v0:
```python
import jax
import jax.numpy as jnp
from jax import lax
from jax.sharding import PartitionSpec as P

HD = 128
SPAN = 128
RBLOCK = 64
NPB = 4
PROWS = 128
eps = 1e-06


def split_up(x, dim, size):
    lengths = x.shape
    parts = x.reshape(*lengths[:dim], size, lengths[dim] // size, *lengths[dim + 1 :])
    return jnp.moveaxis(parts, dim, 0)


def summed_on_arrival(x, axis, dim):
    parts = split_up(x, dim, lax.axis_size(axis))
    arrived = lax.all_to_all(parts, axis, split_axis=0, concat_axis=0, tiled=True)
    return arrived.astype(jnp.float32).sum(axis=0)


def row_norm(values_in, gain):
    widened = values_in.astype(jnp.float32)
    return (
        widened * lax.rsqrt(jnp.mean(widened * widened, axis=-1, keepdims=True) + eps) * gain
    ).astype(jnp.bfloat16)


def local(
    tokens,
    pre_gain,
    w_gated,
    w_mixed,
    mix_weight,
    w_query,
    w_gate_mix,
    w_gate_read,
    store,
    mem_gain,
    w_key,
    w_value,
    passage_ids,
    w_out_mix,
    w_out_read,
):
    tok_rows = tokens.shape[0]
    st_count = lax.axis_size("st")
    normed = row_norm(tokens, pre_gain)
    gated = jnp.dot(normed, w_gated, preferred_element_type=jnp.float32)
    mixed_in = jnp.dot(normed, w_mixed, preferred_element_type=jnp.float32)
    groups_here = mix_weight.shape[0]
    group_width = mixed_in.shape[1] // groups_here
    grouped = mixed_in.reshape(tok_rows, groups_here, group_width)
    group_mean = jnp.mean(grouped, axis=-1, keepdims=True)
    centred = grouped - group_mean
    group_var = jnp.mean(centred * centred, axis=-1, keepdims=True)
    mixed_norm = (centred * lax.rsqrt(group_var + eps)).astype(jnp.bfloat16)
    causal = jnp.tril(jnp.ones((SPAN, SPAN), dtype=bool))
    mix_masked = jnp.where(causal[None], mix_weight, jnp.zeros_like(mix_weight))
    blocked = mixed_norm.reshape(tok_rows // SPAN, SPAN, groups_here, group_width)
    spatial = jnp.einsum(
        "hts,nshd->nthd", mix_masked, blocked, preferred_element_type=jnp.float32
    ).reshape(tok_rows, -1)
    branch_mix = gated * spatial
    query = jnp.dot(normed, w_query, preferred_element_type=jnp.float32).astype(jnp.bfloat16)
    head_width = w_query.shape[1]
    heads_here = head_width // HD
    flat_ids = passage_ids.reshape(-1)
    req_count = flat_ids.shape[0]
    per_owner = store.shape[0]
    capacity = max(2, (2 * req_count + st_count - 1) // st_count)
    owner = flat_ids // per_owner
    local_id = flat_ids - owner * per_owner
    position = jnp.arange(req_count, dtype=jnp.int32)
    same_owner = owner[:, None] == owner[None, :]
    earlier = position[None, :] < position[:, None]
    rank = jnp.sum((same_owner & earlier).astype(jnp.int32), axis=1)
    slot = owner * capacity + rank
    slot_range = jnp.arange(st_count * capacity, dtype=jnp.int32)
    table = jnp.sum(jnp.where(slot[:, None] == slot_range[None, :], local_id[:, None], 0), axis=0)
    table = table.reshape(st_count, capacity)
    held_rows = row_norm(store, mem_gain).reshape(-1, store.shape[-1])
    key_store = (
        jnp.dot(held_rows, w_key, preferred_element_type=jnp.float32)
        .astype(jnp.bfloat16)
        .reshape(per_owner, PROWS, head_width)
    )
    value_store = (
        jnp.dot(held_rows, w_value, preferred_element_type=jnp.float32)
        .astype(jnp.bfloat16)
        .reshape(per_owner, PROWS, head_width)
    )
    wanted = lax.all_to_all(table, "st", split_axis=0, concat_axis=0, tiled=True)
    arrived = (
        lax.all_to_all(key_store[wanted], "st", split_axis=0, concat_axis=0, tiled=True),
        lax.all_to_all(value_store[wanted], "st", split_axis=0, concat_axis=0, tiled=True),
    )
    blocks_here = tok_rows // RBLOCK
    key_slots, value_slots = arrived
    keys = key_slots.reshape(st_count * capacity, PROWS, head_width)[slot]
    values = value_slots.reshape(st_count * capacity, PROWS, head_width)[slot]
    keys = keys.reshape(blocks_here, NPB * PROWS, heads_here, HD)
    values = values.reshape(blocks_here, NPB * PROWS, heads_here, HD)
    query_blocks = query.reshape(blocks_here, RBLOCK, heads_here, HD)
    scores = jnp.einsum(
        "btha,bkha->bhtk", query_blocks, keys, preferred_element_type=jnp.float32
    ) * HD ** (-0.5)
    probs = jax.nn.softmax(scores, axis=-1).astype(jnp.bfloat16)
    branch_read = jnp.einsum(
        "bhtk,bkha->btha", probs, values, preferred_element_type=jnp.float32
    ).reshape(tok_rows, head_width)
    gate_mix = jnp.dot(normed, w_gate_mix, preferred_element_type=jnp.float32)
    gate_read = jnp.dot(normed, w_gate_read, preferred_element_type=jnp.float32)
    out_mix = (branch_mix * jax.nn.silu(gate_mix)).astype(jnp.bfloat16)
    out_read = (branch_read * jax.nn.silu(gate_read)).astype(jnp.bfloat16)
    summed = summed_on_arrival(
        (
            jnp.dot(out_mix, w_out_mix, preferred_element_type=jnp.float32)
            + jnp.dot(out_read, w_out_read, preferred_element_type=jnp.float32)
        ).astype(jnp.bfloat16),
        "tp",
        0,
    )
    return summed.astype(jnp.bfloat16)


def solution(mesh):
    placed = (
        P(("grp", "st"), None),
        P(),
        P(None, "tp"),
        P(None, "tp"),
        P("tp", None, None),
        P(None, "tp"),
        P(None, "tp"),
        P(None, "tp"),
        P(("grp", "st"), None, None),
        P(),
        P(None, "tp"),
        P(None, "tp"),
        P(("grp", "st"), None),
        P("tp", None),
        P("tp", None),
    )
    return jax.shard_map(
        local, mesh=mesh, in_specs=placed, out_specs=P(("grp", "st", "tp"), None), check_vma=False
    )
```

profile of v0, /device:TPU:513, one launch (start us, length us, event | category | flops | bytes accessed | tf_op | source)
XLA Modules:
  0.0 140.8 jit_solution(3696719735241878890)
XLA Ops:
  0.0 0.8 reshape.317
  0.9 0.2 convert_reduce_fusion
  1.1 0.7 all_to_all.17
  1.8 23.7 %all-to-all-start = ((s32[16,1,2]{2,1,0:T(1,128)}), s32[16,1,2]{2,1,0:T(1,128)S(1)}, u32[]{:S(2)}, u32[]{:S(2)}) async-start(s32[16,1,2]{2,1,0:T(1,128)} %bitcast.6), calls=%async_computation | async-start | bytes 16384 | tf_op jit(solution)/shard_map/all_to_all | solution.py:97
  25.5 3.2 %fusion.1 = f32[8,128]{1,0:T(8,128)S(1)} fusion(bf16[8,128,2048]{2,1,0:T(8,128)(2,1)} %param.23), kind=kLoop, calls=%fused_computation.7 | loop fusion | flops 6290432 | bytes 4198400 | tf_op jit(solution)/shard_map/reduce_sum | solution.py:29
  28.8 0.2 copy-done.1
  29.0 1.0 fusion.3
  30.0 1.9 %copy-done.2 = bf16[8,128,2048]{2,1,0:T(8,128)(2,1)} copy-done((bf16[8,128,2048]{2,1,0:T(8,128)(2,1)}, bf16[8,128,2048]{2,1,0:T(8,128)(2,1)S(1)}, u32[]{:S(2)}) %copy-start.2) | copy-done | bytes 4194328
  31.9 1.2 convolution_convert_fusion
  33.5 1.7 %gather_fusion.2 = bf16[32,128,128]{2,1,0:T(8,128)(2,1)} fusion(bf16[8,128,128]{2,1,0:T(8,128)(2,1)S(1)} %bitcast.74, s32[1024]{0:T(1024)S(1)} %pad_clamp_fusion.1), kind=kCustom, calls=%fused_computation.2 | custom fusion | bytes 2097280 | tf_op jit(solution)/shard_map/gather | solution.py:99
  35.2 7.5 %all-to-all-start.2 = ((bf16[16,2,128,128]{3,2,1,0:T(8,128)(2,1)}), bf16[16,2,128,128]{3,2,1,0:T(8,128)(2,1)S(1)}, u32[]{:S(2)}, u32[]{:S(2)}) async-start(bf16[16,2,128,128]{3,2,1,0:T(8,128)(2,1)} %bitcast.15), calls=%async_computation.2 | async-start | bytes 2097152 | tf_op jit(solution)/shard_map/all_to_all | solution.py:99
  42.7 0.3 fusion.5
  43.1 1.7 %fusion.46 = (f32[256]{0:T(256)S(1)}, f32[256,192]{0,1:T(8,128)S(1)}) fusion(bf16[2048,192]{0,1:T(8,128)(2,1)} %param.18, bf16[256,2048]{1,0:T(8,128)(2,1)S(1)} %copy-done.3, f32[2048]{0:T(1024)S(1)} %copy-done.8, f32[256]{0:T(256)S(1)} %add_rsqrt_fusion.2), kind=kOutput, calls=%fused_computation.80 | convolution fusion | flops 203472640 | bytes 2041856 | tf_op jit(solution)/shard_map/dot_general | solution.py:54
  44.8 3.4 %convolution_convert_fusion.1 = bf16[1024,128]{1,0:T(8,128)(2,1)S(1)} fusion(bf16[1024,2048]{1,0:T(8,128)(2,1)} %bitcast.73, bf16[2048,128]{1,0:T(8,128)(2,1)S(1)} %copy-done.12), kind=kOutput, calls=%fused_computation.21 | convolution fusion | flops 537001984 | bytes 4980736 | tf_op jit(solution)/shard_map/dot_general | solution.py:93
  48.3 1.7 %gather_fusion = bf16[32,128,128]{2,1,0:T(8,128)(2,1)} fusion(bf16[8,128,128]{2,1,0:T(8,128)(2,1)S(1)} %bitcast.75, s32[1024]{0:T(1024)S(1)} %pad_clamp_fusion.1), kind=kCustom, calls=%fused_computation | custom fusion | bytes 2097280 | tf_op jit(solution)/shard_map/gather | solution.py:100
  50.0 20.7 %all-to-all-done.2 = bf16[16,2,128,128]{3,2,1,0:T(8,128)(2,1)S(1)} async-done(((bf16[16,2,128,128]{3,2,1,0:T(8,128)(2,1)}), bf16[16,2,128,128]{3,2,1,0:T(8,128)(2,1)S(1)}, u32[]{:S(2)}, u32[]{:S(2)}) %all-to-all-start.2) | async-done | bytes 1048608 | tf_op jit(solution)/shard_map/all_to_all | solution.py:99
  70.6 4.4 %all-to-all-start.1 = ((bf16[16,2,128,128]{3,2,1,0:T(8,128)(2,1)}), bf16[16,2,128,128]{3,2,1,0:T(8,128)(2,1)}, u32[]{:S(2)}, u32[]{:S(2)}) async-start(bf16[16,2,128,128]{3,2,1,0:T(8,128)(2,1)} %bitcast.8), calls=%async_computation.1 | async-start | bytes 2097152 | tf_op jit(solution)/shard_map/all_to_all | solution.py:100
  75.1 0.2 convolution_bitcast_fusion
  75.3 0.2 copy.29
  75.5 2.2 %convolution_convert_fusion.2 = bf16[256,128]{1,0:T(8,128)(2,1)} fusion(bf16[2048,128]{1,0:T(8,128)(2,1)} %param.20, bf16[256,2048]{1,0:T(8,128)(2,1)S(1)} %copy-done.3, f32[2048]{0:T(1024)S(1)} %copy-done.8, f32[256]{0:T(256)S(1)} %add_rsqrt_fusion.2), kind=kOutput, calls=%fused_computation.27 | convolution fusion | flops 136347648 | bytes 1647616 | tf_op jit(solution)/shard_map/dot_general | solution.py:69
  77.7 0.6 fusion.38
  78.3 3.0 %fusion.12 = f32[256,2048]{1,0:T(8,128)S(1)} fusion(bf16[192,2048]{1,0:T(8,128)(2,1)S(1)} %copy-done, bf16[2048,192]{0,1:T(8,128)(2,1)} %param.17, f32[24,8,2,128]{3,2,1,0:T(2,128)S(1)} %bitcast.78, f32[256,192]{0,1:T(8,128)S(1)} %fusion.38, bf16[256,2048]{1,0:T(8,128)(2,1)} %param.15, f32[2048]{0:T(1024)S(1)} %copy-done.8, f32[256]{0:T(256)S(1)} %add_rsqrt_fusion.2), kind=kOutput, calls=%fused_computation.26 | convolution fusion | flops 405094400 | bytes 5121024 | tf_op jit(solution)/shard_map/dot_general | solution.py:122
  81.2 2.6 %gather_fusion.3 = bf16[16,128,128]{2,1,0:T(8,128)(2,1)} fusion(bf16[32,128,128]{2,1,0:T(8,128)(2,1)} %bitcast.76, s32[1024]{0:T(1024)S(1)} %pad_clamp_fusion), kind=kCustom, calls=%fused_computation.3 | custom fusion | bytes 1048640 | tf_op jit(solution)/shard_map/gather | solution.py:104
  83.9 1.4 convolution_multiply_fusion
  85.2 0.2 fusion.47
  85.5 16.7 %all-to-all-done.1 = bf16[16,2,128,128]{3,2,1,0:T(8,128)(2,1)} async-done(((bf16[16,2,128,128]{3,2,1,0:T(8,128)(2,1)}), bf16[16,2,128,128]{3,2,1,0:T(8,128)(2,1)}, u32[]{:S(2)}, u32[]{:S(2)}) %all-to-all-start.1) | async-done | bytes 1048608 | tf_op jit(solution)/shard_map/all_to_all | solution.py:100
  102.1 2.6 %gather_fusion.1 = bf16[16,128,128]{2,1,0:T(8,128)(2,1)} fusion(bf16[32,128,128]{2,1,0:T(8,128)(2,1)} %bitcast.9, s32[1024]{0:T(1024)S(1)} %pad_clamp_fusion), kind=kCustom, calls=%fused_computation.1 | custom fusion | bytes 1048640 | tf_op jit(solution)/shard_map/gather | solution.py:105
  104.8 2.3 %fusion.13 = f32[4,128,64]{1,2,0:T(8,128)} fusion(bf16[4,512,128]{2,1,0:T(8,128)(2,1)} %bitcast.79, f32[4,64]{1,0:T(4,128)S(1)} %fusion.47, f32[4,64,512]{2,1,0:T(8,128)S(1)} %convolution_multiply_fusion), kind=kOutput, calls=%fused_computation.29 | convolution fusion | flops 33948416 | bytes 1180672 | tf_op jit(solution)/shard_map/bhtk,bkha->btha/dot_general | solution.py:113
  107.0 2.0 %fusion.21 = bf16[256,128]{1,0:T(8,128)(2,1)S(1)} fusion(f32[4,128,64]{1,2,0:T(8,128)} %fusion.13, bf16[2048,128]{1,0:T(8,128)(2,1)} %param.22, bf16[256,2048]{1,0:T(8,128)(2,1)} %param.15, f32[2048]{0:T(1024)S(1)} %copy-done.8, f32[256]{0:T(256)S(1)} %add_rsqrt_fusion.2), kind=kOutput, calls=%fused_computation.40 | convolution fusion | flops 136511488 | bytes 1778688 | tf_op jit(solution)/shard_map/dot_general | solution.py:117
  109.0 0.4 fusion.4
  109.4 30.6 %all_to_all.27 = bf16[8,32,2048]{2,1,0:T(8,128)(2,1)S(1)} all-to-all(bf16[8,32,2048]{2,1,0:T(8,128)(2,1)S(1)} %bitcast.71), channel_id=1, replica_groups=mesh['grp'=2,'st'=16,'tp'=8] {'tp'}, dimensions={0} | all-to-all | bytes 2097152 | tf_op jit(solution)/shard_map/all_to_all | solution.py:22
  140.0 0.8 reduce_sum.85
  (41 shorter events, 0.6 us)
Async XLA Ops:
  0.0 78.3 %copy-start = (bf16[192,2048]{1,0:T(8,128)(2,1)S(1)}, bf16[192,2048]{1,0:T(8,128)(2,1)}, u32[]{:S(2)}) copy-start(bf16[192,2048]{1,0:T(8,128)(2,1)} %param.28) | copy-start | bytes 2359300
  1.8 31.4 %all-to-all-start = ((s32[16,1,2]{2,1,0:T(1,128)}), s32[16,1,2]{2,1,0:T(1,128)S(1)}, u32[]{:S(2)}, u32[]{:S(2)}) async-start(s32[16,1,2]{2,1,0:T(1,128)} %bitcast.6), calls=%async_computation | async-start | bytes 16384 | tf_op jit(solution)/shard_map/all_to_all | solution.py:97
  25.5 3.4 %copy-start.1 = (bf16[8,128,2048]{2,1,0:T(8,128)(2,1)S(1)}, bf16[8,128,2048]{2,1,0:T(8,128)(2,1)}, u32[]{:S(2)}) copy-start(bf16[8,128,2048]{2,1,0:T(8,128)(2,1)} %param.23) | copy-start | bytes 12582916
  25.5 3.4 %copy-start.7 = (f32[2048]{0:T(1024)S(1)}, f32[2048]{0:T(1024)}, u32[]{:S(2)}) copy-start(f32[2048]{0:T(1024)} %param.24) | copy-start | bytes 24580
  29.0 3.0 %copy-start.11 = (bf16[2048,128]{1,0:T(8,128)(2,1)S(1)}, bf16[2048,128]{1,0:T(8,128)(2,1)}, u32[]{:S(2)}) copy-start(bf16[2048,128]{1,0:T(8,128)(2,1)} %param.25) | copy-start | bytes 1572868
  30.0 1.9 %copy-start.2 = (bf16[8,128,2048]{2,1,0:T(8,128)(2,1)}, bf16[8,128,2048]{2,1,0:T(8,128)(2,1)S(1)}, u32[]{:S(2)}) copy-start(bf16[8,128,2048]{2,1,0:T(8,128)(2,1)S(1)} %fusion.3) | copy-start | bytes 12582916
  33.5 9.2 %copy-start.9 = (s32[4,4]{1,0:T(4,128)S(1)}, s32[4,4]{1,0:T(4,128)}, u32[]{:S(2)}) copy-start(s32[4,4]{1,0:T(4,128)} %param.27) | copy-start | bytes 196
  33.5 9.3 %copy-start.3 = (bf16[256,2048]{1,0:T(8,128)(2,1)S(1)}, bf16[256,2048]{1,0:T(8,128)(2,1)}, u32[]{:S(2)}) copy-start(bf16[256,2048]{1,0:T(8,128)(2,1)} %param.15) | copy-start | bytes 3145732
  35.1 7.9 %copy-start.8 = (f32[2048]{0:T(1024)S(1)}, f32[2048]{0:T(1024)}, u32[]{:S(2)}) copy-start(f32[2048]{0:T(1024)} %param.16) | copy-start | bytes 24580
  35.2 35.5 %all-to-all-start.2 = ((bf16[16,2,128,128]{3,2,1,0:T(8,128)(2,1)}), bf16[16,2,128,128]{3,2,1,0:T(8,128)(2,1)S(1)}, u32[]{:S(2)}, u32[]{:S(2)}) async-start(bf16[16,2,128,128]{3,2,1,0:T(8,128)(2,1)} %bitcast.15), calls=%async_computation.2 | async-start | bytes 2097152 | tf_op jit(solution)/shard_map/all_to_all | solution.py:99
  42.7 2.1 %copy-start.12 = (bf16[2048,128]{1,0:T(8,128)(2,1)S(1)}, bf16[2048,128]{1,0:T(8,128)(2,1)}, u32[]{:S(2)}) copy-start(bf16[2048,128]{1,0:T(8,128)(2,1)} %param.26) | copy-start | bytes 1572868
  48.3 26.8 %copy-start.6 = (bf16[1,128,128]{2,1,0:T(8,128)(2,1)S(1)}, bf16[1,128,128]{2,1,0:T(8,128)(2,1)}, u32[]{:S(2)}) copy-start(bf16[1,128,128]{2,1,0:T(8,128)(2,1)} %param.19) | copy-start | bytes 98308
  70.6 7.0 %copy-start.4 = (bf16[16,2,128,128]{3,2,1,0:T(8,128)(2,1)}, bf16[16,2,128,128]{3,2,1,0:T(8,128)(2,1)S(1)}, u32[]{:S(2)}) copy-start(bf16[16,2,128,128]{3,2,1,0:T(8,128)(2,1)S(1)} %all-to-all-done.2) | copy-start | bytes 3145732
  70.6 31.5 %all-to-all-start.1 = ((bf16[16,2,128,128]{3,2,1,0:T(8,128)(2,1)}), bf16[16,2,128,128]{3,2,1,0:T(8,128)(2,1)}, u32[]{:S(2)}, u32[]{:S(2)}) async-start(bf16[16,2,128,128]{3,2,1,0:T(8,128)(2,1)} %bitcast.8), calls=%async_computation.1 | async-start | bytes 2097152 | tf_op jit(solution)/shard_map/all_to_all | solution.py:100
  75.1 2.6 %copy-start.10 = (bf16[2048,192]{0,1:T(8,128)(2,1)S(1)}, bf16[2048,192]{0,1:T(8,128)(2,1)}, u32[]{:S(2)}) copy-start(bf16[2048,192]{0,1:T(8,128)(2,1)} %param.21) | copy-start | bytes 2359300
  107.0 2.0 %copy-start.5 = (bf16[128,2048]{1,0:T(8,128)(2,1)S(1)}, bf16[128,2048]{1,0:T(8,128)(2,1)}, u32[]{:S(2)}) copy-start(bf16[128,2048]{1,0:T(8,128)(2,1)} %param.29) | copy-start | bytes 1572868
where the time goes:
time: 141 us
  waiting for transfers between devices  37.3 us (26%)
  starting transfers between devices  35.6 us (25%)
  blocking collectives  30.6 us (22%)
  matrix products  18.3 us (13%)
  local copies, waits for them, and re-layouts  12.8 us (9%)
  other arithmetic  5.97 us (4%)
    all_to_all x1, blocking collectives, summed_on_arrival(): lax.all_to_all(parts, axis, split_axis=0, concat_axis=0, tiled=True)  30.6 us
    all_to_all x1, starting transfers between devices, local(): lax.all_to_all(table, 'st', split_axis=0, concat_axis=0, tiled=True)  23.7 us
    all_to_all x1, waiting for transfers between devices, local(): lax.all_to_all(key_store[wanted], 'st', split_axis=0, concat_axis=0, tile...  20.7 us
    all_to_all x1, waiting for transfers between devices, local(): lax.all_to_all(value_store[wanted], 'st', split_axis=0, concat_axis=0, ti...  16.7 us
    all_to_all x1, starting transfers between devices, local(): lax.all_to_all(key_store[wanted], 'st', split_axis=0, concat_axis=0, tile...  7.5 us
    all_to_all x1, starting transfers between devices, local(): lax.all_to_all(value_store[wanted], 'st', split_axis=0, concat_axis=0, ti...  4.44 us
    reduce_sum x2, other arithmetic, row_norm(): jnp.mean(widened * widened, axis=-1, keepdims=True) + eps  3.51 us
    dot_general x1, matrix products, local(): jnp.dot(held_rows, w_value, preferred_element_type=jnp.float32)  3.44 us
  transfers between devices with their start and end apart: 3, of which 2 were waited for; matrix products, arithmetic and copies ran while one was open for 16% of the time, Pallas kernels for 0%

commit v1 on v0

--- a/solution.py
+++ b/solution.py
@@ -2,6 +2,7 @@
 import jax.numpy as jnp
 from jax import lax
 from jax.sharding import PartitionSpec as P
+from jax.lax import axis_index, axis_size, ppermute
 
 HD = 128
 SPAN = 128
@@ -94,7 +95,21 @@
         .astype(jnp.bfloat16)
         .reshape(per_owner, PROWS, head_width)
     )
-    wanted = lax.all_to_all(table, "st", split_axis=0, concat_axis=0, tiled=True)
+    newest = axis_size("st")
+    x_new, w2 = (newest, axis_index("st"))
+    met_up = table.shape[0] // x_new
+    aux = list(table.shape)
+    aux[0] = met_up
+    reply = aux[0]
+    aux[0] = reply * x_new
+    wanted = jnp.zeros(aux, table.dtype)
+    at = 0
+    while at < x_new:
+        all_rows = lax.dynamic_slice_in_dim(table, (w2 ^ at) * met_up, met_up, axis=0)
+        if at:
+            all_rows = ppermute(all_rows, "st", [(idx, idx ^ at) for idx in range(x_new)])
+        wanted = lax.dynamic_update_slice_in_dim(wanted, all_rows, (w2 ^ at) * reply, axis=0)
+        at += 1
     arrived = (
         lax.all_to_all(key_store[wanted], "st", split_axis=0, concat_axis=0, tiled=True),
         lax.all_to_all(value_store[wanted], "st", split_axis=0, concat_axis=0, tiled=True),

time: 141 us -> 164 us (1.16)
  starting transfers between devices: 35.6 us -> 56.7 us
  other arithmetic: 5.97 us -> 8.07 us
  local copies, waits for them, and re-layouts: 12.8 us -> 11.1 us
    ppermute x0 -> x15, starting transfers between devices: none -> 46.9 us  [local(): ppermute(all_rows, 'st', [(idx, idx ^ at) for idx in range(x_new)])]
    all_to_all x1 -> x0, starting transfers between devices: 23.7 us -> none  [local(): lax.all_to_all(table, 'st', split_axis=0, concat_axis=0, tiled=True)]
    convert_element_type x1, other arithmetic: 1.02 us -> 3.27 us  [row_norm(): return (widened * lax.rsqrt(jnp.mean(widened * widened, axis=-1, keepdims...]
    all_to_all x1, starting transfers between devices: 7.5 us -> 5.38 us  [local(): lax.all_to_all(key_store[wanted], 'st', split_axis=0, concat_axis=0, tile...]
  transfers between devices with their start and end apart: 3 -> 17, of which waited for: 2 -> 4; matrix products, arithmetic and copies ran while one was open for 16% -> 16% of each run, Pallas kernels for 0% -> 0%
where the time goes in v1:
time: 164 us
  starting transfers between devices  56.7 us (35%)
  waiting for transfers between devices  38.5 us (23%)
  blocking collectives  30.6 us (19%)
  matrix products  18.3 us (11%)
  local copies, waits for them, and re-layouts  11.1 us (7%)
  other arithmetic  8.07 us (5%)
    ppermute x15, starting transfers between devices, local(): ppermute(all_rows, 'st', [(idx, idx ^ at) for idx in range(x_new)])  46.9 us
    all_to_all x1, blocking collectives, summed_on_arrival(): lax.all_to_all(parts, axis, split_axis=0, concat_axis=0, tiled=True)  30.6 us
    all_to_all x1, waiting for transfers between devices, local(): lax.all_to_all(key_store[wanted], 'st', split_axis=0, concat_axis=0, tile...  20.7 us
    all_to_all x1, waiting for transfers between devices, local(): lax.all_to_all(value_store[wanted], 'st', split_axis=0, concat_axis=0, ti...  16.6 us
    all_to_all x1, starting transfers between devices, local(): lax.all_to_all(key_store[wanted], 'st', split_axis=0, concat_axis=0, tile...  5.38 us
    all_to_all x1, starting transfers between devices, local(): lax.all_to_all(value_store[wanted], 'st', split_axis=0, concat_axis=0, ti...  4.45 us
    dot_general x1, matrix products, local(): jnp.dot(held_rows, w_value, preferred_element_type=jnp.float32)  3.44 us
    reduce_sum x2, other arithmetic, row_norm(): jnp.mean(widened * widened, axis=-1, keepdims=True) + eps  3.36 us
  transfers between devices with their start and end apart: 17, of which 4 were waited for; matrix products, arithmetic and copies ran while one was open for 16% of the time, Pallas kernels for 0%

profile of v1, /device:TPU:513, one launch (start us, length us, event | category | flops | bytes accessed | tf_op | source)
XLA Modules:
  0.0 163.6 jit_solution(18165602198646006598)
XLA Ops:
  0.0 0.8 reshape.288
  1.4 20.5 %collective-permute-start = (s32[1,2]{1,0:T(1,128)S(1)}, s32[1,2]{1,0:T(1,128)S(1)}, u32[]{:S(2)}, u32[]{:S(2)}) collective-permute-start(s32[1,2]{1,0:T(1,128)S(1)} %get-tuple-element.21), channel_id=1, source_target_pairs={{0,8},{8,0},{16,24},{24,16},{32,40},{40,32},{48,56},{56,48},{64,72... | collective-permute-start | bytes 32 | tf_op jit(solution)/shard_map/ppermute | solution.py:110
  21.9 1.8 %collective-permute-start.2 = (s32[1,2]{1,0:T(1,128)S(1)}, s32[1,2]{1,0:T(1,128)S(1)}, u32[]{:S(2)}, u32[]{:S(2)}) collective-permute-start(s32[1,2]{1,0:T(1,128)S(1)} %get-tuple-element.19), channel_id=1, source_target_pairs={{0,24},{8,16},{16,8},{24,0},{32,56},{40,48},{48,40},{56,32},{64,88... | collective-permute-start | bytes 32 | tf_op jit(solution)/shard_map/ppermute | solution.py:110
  23.7 2.6 %collective-permute-start.4 = (s32[1,2]{1,0:T(1,128)S(1)}, s32[1,2]{1,0:T(1,128)S(1)}, u32[]{:S(2)}, u32[]{:S(2)}) collective-permute-start(s32[1,2]{1,0:T(1,128)S(1)} %get-tuple-element.17), channel_id=1, source_target_pairs={{0,40},{8,32},{16,56},{24,48},{32,8},{40,0},{48,24},{56,16},{64,10... | collective-permute-start | bytes 32 | tf_op jit(solution)/shard_map/ppermute | solution.py:110
  26.3 3.1 %fusion.1 = f32[8,128]{1,0:T(8,128)S(1)} fusion(bf16[8,128,2048]{2,1,0:T(8,128)(2,1)} %param.23), kind=kLoop, calls=%fused_computation.7 | loop fusion | flops 6290432 | bytes 4198400 | tf_op jit(solution)/shard_map/reduce_sum | solution.py:30
  29.4 3.3 %fusion.3 = bf16[8,128,2048]{2,1,0:T(8,128)(2,1)S(1)} fusion(bf16[8,128,2048]{2,1,0:T(8,128)(2,1)} %param.23, f32[2048]{0:T(1024)S(1)} %copy-done.6, f32[8,128]{1,0:T(8,128)S(1)} %add_rsqrt_fusion), kind=kLoop, calls=%fused_computation.9 | loop fusion | flops 8388608 | bytes 8400896 | tf_op jit(solution)/shard_map/convert_element_type | solution.py:31
  32.7 1.2 convolution_convert_fusion
  34.0 0.7 copy-done.1
  34.7 3.7 %collective-permute-start.6 = (s32[1,2]{1,0:T(1,128)S(1)}, s32[1,2]{1,0:T(1,128)S(1)}, u32[]{:S(2)}, u32[]{:S(2)}) collective-permute-start(s32[1,2]{1,0:T(1,128)S(1)} %get-tuple-element.15), channel_id=1, source_target_pairs={{0,56},{8,48},{16,40},{24,32},{32,24},{40,16},{48,8},{56,0},{64,12... | collective-permute-start | bytes 32 | tf_op jit(solution)/shard_map/ppermute | solution.py:110
  38.6 5.7 %collective-permute-start.8 = (s32[1,2]{1,0:T(1,128)S(1)}, s32[1,2]{1,0:T(1,128)S(1)}, u32[]{:S(2)}, u32[]{:S(2)}) collective-permute-start(s32[1,2]{1,0:T(1,128)S(1)} %get-tuple-element.13), channel_id=1, source_target_pairs={{0,72},{8,64},{16,88},{24,80},{32,104},{40,96},{48,120},{56,112},{... | collective-permute-start | bytes 32 | tf_op jit(solution)/shard_map/ppermute | solution.py:110
  44.5 4.9 %collective-permute-start.10 = (s32[1,2]{1,0:T(1,128)S(1)}, s32[1,2]{1,0:T(1,128)S(1)}, u32[]{:S(2)}, u32[]{:S(2)}) collective-permute-start(s32[1,2]{1,0:T(1,128)S(1)} %get-tuple-element.11), channel_id=1, source_target_pairs={{0,88},{8,80},{16,72},{24,64},{32,120},{40,112},{48,104},{56,96},{... | collective-permute-start | bytes 32 | tf_op jit(solution)/shard_map/ppermute | solution.py:110
  49.6 3.9 %collective-permute-start.12 = (s32[1,2]{1,0:T(1,128)S(1)}, s32[1,2]{1,0:T(1,128)S(1)}, u32[]{:S(2)}, u32[]{:S(2)}) collective-permute-start(s32[1,2]{1,0:T(1,128)S(1)} %get-tuple-element.9), channel_id=1, source_target_pairs={{0,104},{8,96},{16,120},{24,112},{32,72},{40,64},{48,88},{56,80},{... | collective-permute-start | bytes 32 | tf_op jit(solution)/shard_map/ppermute | solution.py:110
  53.7 3.2 %collective-permute-start.14 = (s32[1,2]{1,0:T(1,128)S(1)}, s32[1,2]{1,0:T(1,128)S(1)}, u32[]{:S(2)}, u32[]{:S(2)}) collective-permute-start(s32[1,2]{1,0:T(1,128)S(1)} %get-tuple-element.7), channel_id=1, source_target_pairs={{0,120},{8,112},{16,104},{24,96},{32,88},{40,80},{48,72},{56,64},{... | collective-permute-start | bytes 32 | tf_op jit(solution)/shard_map/ppermute | solution.py:110
  57.3 0.9 collective-permute-done.14
  58.4 1.7 %gather_fusion.2 = bf16[32,128,128]{2,1,0:T(8,128)(2,1)} fusion(bf16[8,128,128]{2,1,0:T(8,128)(2,1)S(1)} %bitcast.69, s32[1024]{0:T(1024)S(1)} %pad_clamp_fusion.1), kind=kCustom, calls=%fused_computation.2 | custom fusion | bytes 2097280 | tf_op jit(solution)/shard_map/gather | solution.py:114
  60.1 5.4 %all-to-all-start.1 = ((bf16[16,2,128,128]{3,2,1,0:T(8,128)(2,1)}), bf16[16,2,128,128]{3,2,1,0:T(8,128)(2,1)S(1)}, u32[]{:S(2)}, u32[]{:S(2)}) async-start(bf16[16,2,128,128]{3,2,1,0:T(8,128)(2,1)} %bitcast.13), calls=%async_computation.1 | async-start | bytes 2097152 | tf_op jit(solution)/shard_map/all_to_all | solution.py:114
  65.8 1.7 %fusion.46 = (f32[256]{0:T(256)S(1)}, f32[256,192]{0,1:T(8,128)S(1)}) fusion(bf16[2048,192]{0,1:T(8,128)(2,1)} %param.18, bf16[256,2048]{1,0:T(8,128)(2,1)S(1)} %copy-done.2, f32[2048]{0:T(1024)S(1)} %copy-done.7, f32[256]{0:T(256)S(1)} %add_rsqrt_fusion.2), kind=kOutput, calls=%fused_computation.96 | convolution fusion | flops 203472640 | bytes 2041856 | tf_op jit(solution)/shard_map/dot_general | solution.py:55
  67.6 3.4 %convolution_convert_fusion.1 = bf16[1024,128]{1,0:T(8,128)(2,1)S(1)} fusion(bf16[1024,2048]{1,0:T(8,128)(2,1)} %bitcast.68, bf16[2048,128]{1,0:T(8,128)(2,1)S(1)} %copy-done.11), kind=kOutput, calls=%fused_computation.21 | convolution fusion | flops 537001984 | bytes 4980736 | tf_op jit(solution)/shard_map/dot_general | solution.py:94
  71.1 1.6 %gather_fusion = bf16[32,128,128]{2,1,0:T(8,128)(2,1)} fusion(bf16[8,128,128]{2,1,0:T(8,128)(2,1)S(1)} %bitcast.70, s32[1024]{0:T(1024)S(1)} %pad_clamp_fusion.1), kind=kCustom, calls=%fused_computation | custom fusion | bytes 2097280 | tf_op jit(solution)/shard_map/gather | solution.py:115
  72.7 20.7 %all-to-all-done.1 = bf16[16,2,128,128]{3,2,1,0:T(8,128)(2,1)S(1)} async-done(((bf16[16,2,128,128]{3,2,1,0:T(8,128)(2,1)}), bf16[16,2,128,128]{3,2,1,0:T(8,128)(2,1)S(1)}, u32[]{:S(2)}, u32[]{:S(2)}) %all-to-all-start.1) | async-done | bytes 1048608 | tf_op jit(solution)/shard_map/all_to_all | solution.py:114
  93.4 4.4 %all-to-all-start = ((bf16[16,2,128,128]{3,2,1,0:T(8,128)(2,1)}), bf16[16,2,128,128]{3,2,1,0:T(8,128)(2,1)}, u32[]{:S(2)}, u32[]{:S(2)}) async-start(bf16[16,2,128,128]{3,2,1,0:T(8,128)(2,1)} %bitcast.6), calls=%async_computation | async-start | bytes 2097152 | tf_op jit(solution)/shard_map/all_to_all | solution.py:115
  98.3 2.2 %convolution_convert_fusion.2 = bf16[256,128]{1,0:T(8,128)(2,1)} fusion(bf16[2048,128]{1,0:T(8,128)(2,1)} %param.20, bf16[256,2048]{1,0:T(8,128)(2,1)S(1)} %copy-done.2, f32[2048]{0:T(1024)S(1)} %copy-done.7, f32[256]{0:T(256)S(1)} %add_rsqrt_fusion.2), kind=kOutput, calls=%fused_computation.27 | convolution fusion | flops 136347648 | bytes 1647616 | tf_op jit(solution)/shard_map/dot_general | solution.py:70
  100.5 0.6 fusion.38
  101.1 3.0 %fusion.12 = f32[256,2048]{1,0:T(8,128)S(1)} fusion(bf16[192,2048]{1,0:T(8,128)(2,1)S(1)} %copy-done, bf16[2048,192]{0,1:T(8,128)(2,1)} %param.17, f32[24,8,2,128]{3,2,1,0:T(2,128)S(1)} %bitcast.73, f32[256,192]{0,1:T(8,128)S(1)} %fusion.38, bf16[256,2048]{1,0:T(8,128)(2,1)} %param.15, f32[2048]{0:T(1024)S(1)} %copy-done.7, f32[256]{0:T(256)S(1)} %add_rsqrt_fusion.2), kind=kOutput, calls=%fused_computation.26 | convolution fusion | flops 405094400 | bytes 5121024 | tf_op jit(solution)/shard_map/dot_general | solution.py:137
  104.0 2.6 %gather_fusion.3 = bf16[16,128,128]{2,1,0:T(8,128)(2,1)} fusion(bf16[32,128,128]{2,1,0:T(8,128)(2,1)} %bitcast.71, s32[1024]{0:T(1024)S(1)} %pad_clamp_fusion), kind=kCustom, calls=%fused_computation.3 | custom fusion | bytes 1048640 | tf_op jit(solution)/shard_map/gather | solution.py:119
  106.7 1.4 convolution_multiply_fusion
  108.3 16.6 %all-to-all-done = bf16[16,2,128,128]{3,2,1,0:T(8,128)(2,1)} async-done(((bf16[16,2,128,128]{3,2,1,0:T(8,128)(2,1)}), bf16[16,2,128,128]{3,2,1,0:T(8,128)(2,1)}, u32[]{:S(2)}, u32[]{:S(2)}) %all-to-all-start) | async-done | bytes 1048608 | tf_op jit(solution)/shard_map/all_to_all | solution.py:115
  124.9 2.6 %gather_fusion.1 = bf16[16,128,128]{2,1,0:T(8,128)(2,1)} fusion(bf16[32,128,128]{2,1,0:T(8,128)(2,1)} %bitcast.7, s32[1024]{0:T(1024)S(1)} %pad_clamp_fusion), kind=kCustom, calls=%fused_computation.1 | custom fusion | bytes 1048640 | tf_op jit(solution)/shard_map/gather | solution.py:120
  127.5 2.3 %fusion.13 = f32[4,128,64]{1,2,0:T(8,128)} fusion(bf16[4,512,128]{2,1,0:T(8,128)(2,1)} %bitcast.74, f32[4,64]{1,0:T(4,128)S(1)} %fusion.47, f32[4,64,512]{2,1,0:T(8,128)S(1)} %convolution_multiply_fusion), kind=kOutput, calls=%fused_computation.29 | convolution fusion | flops 33948416 | bytes 1180672 | tf_op jit(solution)/shard_map/bhtk,bkha->btha/dot_general | solution.py:128
  129.8 2.0 %fusion.21 = bf16[256,128]{1,0:T(8,128)(2,1)S(1)} fusion(f32[4,128,64]{1,2,0:T(8,128)} %fusion.13, bf16[2048,128]{1,0:T(8,128)(2,1)} %param.22, bf16[256,2048]{1,0:T(8,128)(2,1)} %param.15, f32[2048]{0:T(1024)S(1)} %copy-done.7, f32[256]{0:T(256)S(1)} %add_rsqrt_fusion.2), kind=kOutput, calls=%fused_computation.40 | convolution fusion | flops 136511488 | bytes 1778688 | tf_op jit(solution)/shard_map/dot_general | solution.py:132
  132.2 30.6 %all_to_all.15 = bf16[8,32,2048]{2,1,0:T(8,128)(2,1)S(1)} all-to-all(bf16[8,32,2048]{2,1,0:T(8,128)(2,1)S(1)} %bitcast.66), channel_id=1, replica_groups=mesh['grp'=2,'st'=16,'tp'=8] {'tp'}, dimensions={0} | all-to-all | bytes 2097152 | tf_op jit(solution)/shard_map/all_to_all | solution.py:23
  162.8 0.8 reduce_sum.85
  (83 shorter events, 3.3 us)
Async XLA Ops:
  0.0 101.1 %copy-start = (bf16[192,2048]{1,0:T(8,128)(2,1)S(1)}, bf16[192,2048]{1,0:T(8,128)(2,1)}, u32[]{:S(2)}) copy-start(bf16[192,2048]{1,0:T(8,128)(2,1)} %param.28) | copy-start | bytes 2359300
  1.4 33.3 %collective-permute-start = (s32[1,2]{1,0:T(1,128)S(1)}, s32[1,2]{1,0:T(1,128)S(1)}, u32[]{:S(2)}, u32[]{:S(2)}) collective-permute-start(s32[1,2]{1,0:T(1,128)S(1)} %get-tuple-element.21), channel_id=1, source_target_pairs={{0,8},{8,0},{16,24},{24,16},{32,40},{40,32},{48,56},{56,48},{64,72... | collective-permute-start | bytes 32 | tf_op jit(solution)/shard_map/ppermute | solution.py:110
  21.9 12.8 %collective-permute-start.1 = (s32[1,2]{1,0:T(1,128)S(1)}, s32[1,2]{1,0:T(1,128)S(1)}, u32[]{:S(2)}, u32[]{:S(2)}) collective-permute-start(s32[1,2]{1,0:T(1,128)S(1)} %get-tuple-element.20), channel_id=1, source_target_pairs={{0,16},{8,24},{16,0},{24,8},{32,48},{40,56},{48,32},{56,40},{64,80... | collective-permute-start | bytes 32 | tf_op jit(solution)/shard_map/ppermute | solution.py:110
  21.9 16.5 %collective-permute-start.2 = (s32[1,2]{1,0:T(1,128)S(1)}, s32[1,2]{1,0:T(1,128)S(1)}, u32[]{:S(2)}, u32[]{:S(2)}) collective-permute-start(s32[1,2]{1,0:T(1,128)S(1)} %get-tuple-element.19), channel_id=1, source_target_pairs={{0,24},{8,16},{16,8},{24,0},{32,56},{40,48},{48,40},{56,32},{64,88... | collective-permute-start | bytes 32 | tf_op jit(solution)/shard_map/ppermute | solution.py:110
  23.7 14.9 %collective-permute-start.3 = (s32[1,2]{1,0:T(1,128)S(1)}, s32[1,2]{1,0:T(1,128)S(1)}, u32[]{:S(2)}, u32[]{:S(2)}) collective-permute-start(s32[1,2]{1,0:T(1,128)S(1)} %get-tuple-element.18), channel_id=1, source_target_pairs={{0,32},{8,40},{16,48},{24,56},{32,0},{40,8},{48,16},{56,24},{64,96... | collective-permute-start | bytes 32 | tf_op jit(solution)/shard_map/ppermute | solution.py:110
  23.7 5.7 %copy-start.6 = (f32[2048]{0:T(1024)S(1)}, f32[2048]{0:T(1024)}, u32[]{:S(2)}) copy-start(f32[2048]{0:T(1024)} %param.24) | copy-start | bytes 24580
  23.7 20.6 %collective-permute-start.4 = (s32[1,2]{1,0:T(1,128)S(1)}, s32[1,2]{1,0:T(1,128)S(1)}, u32[]{:S(2)}, u32[]{:S(2)}) collective-permute-start(s32[1,2]{1,0:T(1,128)S(1)} %get-tuple-element.17), channel_id=1, source_target_pairs={{0,40},{8,32},{16,56},{24,48},{32,8},{40,0},{48,24},{56,16},{64,10... | collective-permute-start | bytes 32 | tf_op jit(solution)/shard_map/ppermute | solution.py:110
  29.4 3.3 %copy-start.10 = (bf16[2048,128]{1,0:T(8,128)(2,1)S(1)}, bf16[2048,128]{1,0:T(8,128)(2,1)}, u32[]{:S(2)}) copy-start(bf16[2048,128]{1,0:T(8,128)(2,1)} %param.25) | copy-start | bytes 1572868
  32.7 1.9 %copy-start.1 = (bf16[8,128,2048]{2,1,0:T(8,128)(2,1)}, bf16[8,128,2048]{2,1,0:T(8,128)(2,1)S(1)}, u32[]{:S(2)}) copy-start(bf16[8,128,2048]{2,1,0:T(8,128)(2,1)S(1)} %fusion.3) | copy-start | bytes 12582916
  34.7 9.9 %collective-permute-start.5 = (s32[1,2]{1,0:T(1,128)S(1)}, s32[1,2]{1,0:T(1,128)S(1)}, u32[]{:S(2)}, u32[]{:S(2)}) collective-permute-start(s32[1,2]{1,0:T(1,128)S(1)} %get-tuple-element.16), channel_id=1, source_target_pairs={{0,48},{8,56},{16,32},{24,40},{32,16},{40,24},{48,0},{56,8},{64,11... | collective-permute-start | bytes 32 | tf_op jit(solution)/shard_map/ppermute | solution.py:110
  34.7 14.7 %collective-permute-start.6 = (s32[1,2]{1,0:T(1,128)S(1)}, s32[1,2]{1,0:T(1,128)S(1)}, u32[]{:S(2)}, u32[]{:S(2)}) collective-permute-start(s32[1,2]{1,0:T(1,128)S(1)} %get-tuple-element.15), channel_id=1, source_target_pairs={{0,56},{8,48},{16,40},{24,32},{32,24},{40,16},{48,8},{56,0},{64,12... | collective-permute-start | bytes 32 | tf_op jit(solution)/shard_map/ppermute | solution.py:110
  38.4 11.2 %collective-permute-start.7 = (s32[1,2]{1,0:T(1,128)S(1)}, s32[1,2]{1,0:T(1,128)S(1)}, u32[]{:S(2)}, u32[]{:S(2)}) collective-permute-start(s32[1,2]{1,0:T(1,128)S(1)} %get-tuple-element.14), channel_id=1, source_target_pairs={{0,64},{8,72},{16,80},{24,88},{32,96},{40,104},{48,112},{56,120},{... | collective-permute-start | bytes 32 | tf_op jit(solution)/shard_map/ppermute | solution.py:110
  38.6 14.9 %collective-permute-start.8 = (s32[1,2]{1,0:T(1,128)S(1)}, s32[1,2]{1,0:T(1,128)S(1)}, u32[]{:S(2)}, u32[]{:S(2)}) collective-permute-start(s32[1,2]{1,0:T(1,128)S(1)} %get-tuple-element.13), channel_id=1, source_target_pairs={{0,72},{8,64},{16,88},{24,80},{32,104},{40,96},{48,120},{56,112},{... | collective-permute-start | bytes 32 | tf_op jit(solution)/shard_map/ppermute | solution.py:110
  44.3 9.4 %collective-permute-start.9 = (s32[1,2]{1,0:T(1,128)S(1)}, s32[1,2]{1,0:T(1,128)S(1)}, u32[]{:S(2)}, u32[]{:S(2)}) collective-permute-start(s32[1,2]{1,0:T(1,128)S(1)} %get-tuple-element.12), channel_id=1, source_target_pairs={{0,80},{8,88},{16,64},{24,72},{32,112},{40,120},{48,96},{56,104},{... | collective-permute-start | bytes 32 | tf_op jit(solution)/shard_map/ppermute | solution.py:110
  44.5 12.5 %collective-permute-start.10 = (s32[1,2]{1,0:T(1,128)S(1)}, s32[1,2]{1,0:T(1,128)S(1)}, u32[]{:S(2)}, u32[]{:S(2)}) collective-permute-start(s32[1,2]{1,0:T(1,128)S(1)} %get-tuple-element.11), channel_id=1, source_target_pairs={{0,88},{8,80},{16,72},{24,64},{32,120},{40,112},{48,104},{56,96},{... | collective-permute-start | bytes 32 | tf_op jit(solution)/shard_map/ppermute | solution.py:110
  49.4 7.6 %collective-permute-start.11 = (s32[1,2]{1,0:T(1,128)S(1)}, s32[1,2]{1,0:T(1,128)S(1)}, u32[]{:S(2)}, u32[]{:S(2)}) collective-permute-start(s32[1,2]{1,0:T(1,128)S(1)} %get-tuple-element.10), channel_id=1, source_target_pairs={{0,96},{8,104},{16,112},{24,120},{32,64},{40,72},{48,80},{56,88},{... | collective-permute-start | bytes 32 | tf_op jit(solution)/shard_map/ppermute | solution.py:110
  49.6 7.5 %collective-permute-start.12 = (s32[1,2]{1,0:T(1,128)S(1)}, s32[1,2]{1,0:T(1,128)S(1)}, u32[]{:S(2)}, u32[]{:S(2)}) collective-permute-start(s32[1,2]{1,0:T(1,128)S(1)} %get-tuple-element.9), channel_id=1, source_target_pairs={{0,104},{8,96},{16,120},{24,112},{32,72},{40,64},{48,88},{56,80},{... | collective-permute-start | bytes 32 | tf_op jit(solution)/shard_map/ppermute | solution.py:110
  53.5 3.7 %collective-permute-start.13 = (s32[1,2]{1,0:T(1,128)S(1)}, s32[1,2]{1,0:T(1,128)S(1)}, u32[]{:S(2)}, u32[]{:S(2)}) collective-permute-start(s32[1,2]{1,0:T(1,128)S(1)} %get-tuple-element.8), channel_id=1, source_target_pairs={{0,112},{8,120},{16,96},{24,104},{32,80},{40,88},{48,64},{56,72},{... | collective-permute-start | bytes 32 | tf_op jit(solution)/shard_map/ppermute | solution.py:110
  53.7 4.5 %collective-permute-start.14 = (s32[1,2]{1,0:T(1,128)S(1)}, s32[1,2]{1,0:T(1,128)S(1)}, u32[]{:S(2)}, u32[]{:S(2)}) collective-permute-start(s32[1,2]{1,0:T(1,128)S(1)} %get-tuple-element.7), channel_id=1, source_target_pairs={{0,120},{8,112},{16,104},{24,96},{32,88},{40,80},{48,72},{56,64},{... | collective-permute-start | bytes 32 | tf_op jit(solution)/shard_map/ppermute | solution.py:110
  58.4 7.1 %copy-start.8 = (s32[4,4]{1,0:T(4,128)S(1)}, s32[4,4]{1,0:T(4,128)}, u32[]{:S(2)}) copy-start(s32[4,4]{1,0:T(4,128)} %param.27) | copy-start | bytes 196
  58.4 7.2 %copy-start.2 = (bf16[256,2048]{1,0:T(8,128)(2,1)S(1)}, bf16[256,2048]{1,0:T(8,128)(2,1)}, u32[]{:S(2)}) copy-start(bf16[256,2048]{1,0:T(8,128)(2,1)} %param.15) | copy-start | bytes 3145732
  60.1 5.8 %copy-start.7 = (f32[2048]{0:T(1024)S(1)}, f32[2048]{0:T(1024)}, u32[]{:S(2)}) copy-start(f32[2048]{0:T(1024)} %param.16) | copy-start | bytes 24580
  60.1 33.4 %all-to-all-start.1 = ((bf16[16,2,128,128]{3,2,1,0:T(8,128)(2,1)}), bf16[16,2,128,128]{3,2,1,0:T(8,128)(2,1)S(1)}, u32[]{:S(2)}, u32[]{:S(2)}) async-start(bf16[16,2,128,128]{3,2,1,0:T(8,128)(2,1)} %bitcast.13), calls=%async_computation.1 | async-start | bytes 2097152 | tf_op jit(solution)/shard_map/all_to_all | solution.py:114
  65.5 2.1 %copy-start.11 = (bf16[2048,128]{1,0:T(8,128)(2,1)S(1)}, bf16[2048,128]{1,0:T(8,128)(2,1)}, u32[]{:S(2)}) copy-start(bf16[2048,128]{1,0:T(8,128)(2,1)} %param.26) | copy-start | bytes 1572868
  71.1 26.8 %copy-start.5 = (bf16[1,128,128]{2,1,0:T(8,128)(2,1)S(1)}, bf16[1,128,128]{2,1,0:T(8,128)(2,1)}, u32[]{:S(2)}) copy-start(bf16[1,128,128]{2,1,0:T(8,128)(2,1)} %param.19) | copy-start | bytes 98308
  93.4 7.0 %copy-start.3 = (bf16[16,2,128,128]{3,2,1,0:T(8,128)(2,1)}, bf16[16,2,128,128]{3,2,1,0:T(8,128)(2,1)S(1)}, u32[]{:S(2)}) copy-start(bf16[16,2,128,128]{3,2,1,0:T(8,128)(2,1)S(1)} %all-to-all-done.1) | copy-start | bytes 3145732
  93.4 31.5 %all-to-all-start = ((bf16[16,2,128,128]{3,2,1,0:T(8,128)(2,1)}), bf16[16,2,128,128]{3,2,1,0:T(8,128)(2,1)}, u32[]{:S(2)}, u32[]{:S(2)}) async-start(bf16[16,2,128,128]{3,2,1,0:T(8,128)(2,1)} %bitcast.6), calls=%async_computation | async-start | bytes 2097152 | tf_op jit(solution)/shard_map/all_to_all | solution.py:115
  97.9 2.6 %copy-start.9 = (bf16[2048,192]{0,1:T(8,128)(2,1)S(1)}, bf16[2048,192]{0,1:T(8,128)(2,1)}, u32[]{:S(2)}) copy-start(bf16[2048,192]{0,1:T(8,128)(2,1)} %param.21) | copy-start | bytes 2359300
  129.8 2.0 %copy-start.4 = (bf16[128,2048]{1,0:T(8,128)(2,1)S(1)}, bf16[128,2048]{1,0:T(8,128)(2,1)}, u32[]{:S(2)}) copy-start(bf16[128,2048]{1,0:T(8,128)(2,1)} %param.29) | copy-start | bytes 1572868
